TPU v7x, 32 devices: a whole 2x2x4 slice. The times are simulated.
32 devices in a mesh: fs: 8 (over z, x), tp: 4 (over y, core).
Axes of the slice: x: 2, y: 2, z: 4, core: 2. Of those that a mesh axis runs over, the one named last changes fastest.
Arguments:
- tokens: bfloat16 [6144, 2048], P('fs', 'tp'), may hold values from -6 to 6
- mix_gain: float32 [2048], replicated, may hold values from 0.1 to 1.9
- outer_gate: bfloat16 [2048, 2048], P('fs', 'tp'), may hold values from -0.125 to 0.125
- inner_gate: bfloat16 [2048, 2048], P('fs', 'tp'), may hold values from -0.125 to 0.125
- signal_in: bfloat16 [2048, 2048], P('fs', 'tp'), may hold values from -0.125 to 0.125
- mix_taps: float32 [3, 2048], P(None, 'tp'), may hold values from -3 to 3
- mix_bias: float32 [2048], P('tp'), may hold values from -3 to 3
- mix_out: bfloat16 [2048, 2048], P('tp', 'fs'), may hold values from -0.1875 to 0.1875
- ffn_gain: float32 [2048], replicated, may hold values from 0.1 to 1.9
- up_gate: bfloat16 [2048, 5632], P('fs', 'tp'), may hold values from -0.125 to 0.125
- up_value: bfloat16 [2048, 5632], P('fs', 'tp'), may hold values from -0.125 to 0.125
- ffn_taps: float32 [2, 3, 5632], P(None, None, 'tp'), may hold values from -3 to 3
- ffn_bias: float32 [2, 5632], P(None, 'tp'), may hold values from -3 to 3
- down_proj: bfloat16 [5632, 2048], P('tp', 'fs'), may hold values from -0.109375 to 0.109375
Outputs:
- layer_out: bfloat16 [6144, 2048], P('fs', 'tp')
All inputs are finite; a program needn't handle non-finite values.
Results may differ from a plain program's by a relative error of at most 0.023.
Values may be sent and summed in bfloat16 or wider, within the bound.
A program may use at most 64 MiB of HBM per device.

v0:
```python
import functools

import jax
import jax.numpy as jnp
from jax import lax
from jax.experimental import pallas as pl
from jax.experimental.pallas import tpu as pltpu
from jax.sharding import PartitionSpec as P

EPS = 1e-06
F32, BF16 = jnp.float32, jnp.bfloat16
MESH = pl.DeviceIdType.MESH
UP, DOWN, RIGHT, LEFT = range(4)


def grid_of(n_fs):
    nx = 1
    while nx * nx * 4 <= n_fs:
        nx *= 2
    return n_fs // nx, nx


def tiles(extent, width, body):
    whole = extent // width
    if whole:
        @pl.loop(0, whole)
        def _(i):
            body(i, pl.multiple_of(i * width, width), width)
    if extent % width:
        body(whole, whole * width, extent % width)


def causal(v, taps, bias):
    row = lax.broadcasted_iota(jnp.int32, v.shape, 0)
    first = jnp.where(row < 1, 0.0, pltpu.roll(v, 1, axis=0))
    second = jnp.where(row < 2, 0.0, pltpu.roll(v, 2, axis=0))
    return taps[2] * v + taps[1] * first + taps[0] * second + bias


def kernel(
    n_fs, n_tp, tok_in, og, ig, si, mo, ug, uv, dp,
    mix_gain, ffn_gain, mix_taps, mix_bias, ffn_taps, ffn_bias,
    out,
    w0, w1, w2, w3, w4, w5, w6,
    tok, normed, state, outer, inner, signal, gate, value,
    part1, rs1, part2, rs2,
    load_sem, send_sem, recv_sem,
    tok_send, tok_recv, st_send, st_recv, p1_send, p1_recv, p2_send, p2_recv,
):
    nz, nx = grid_of(n_fs)
    fs, tp = lax.axis_index("fs"), lax.axis_index("tp")
    z, x = fs // nx, fs % nx
    bufs = (w0, w1, w2, w3, w4, w5, w6)
    sources = (og, ig, si, mo, ug, uv, dp)
    rows, own = tok.shape[1], tok.shape[2]
    per = n_fs // n_tp
    wide = part1.shape[2]

    ways = (
        (z < nz - 1, fs + nx),
        (z > 0, fs - nx),
        (x < nx - 1, fs + 1),
        (x > 0, fs - 1),
    )
    barrier = pltpu.get_barrier_semaphore()
    expected = n_tp - 1
    for there, peer in ways:
        expected = expected + jnp.where(there, 1, 0)

        @pl.when(there)
        def _(peer=peer):
            pl.semaphore_signal(barrier, inc=1, device_id={"fs": peer}, device_id_type=MESH)
    peers = [(tp + r) % n_tp for r in range(1, n_tp)]
    for peer in peers:
        pl.semaphore_signal(barrier, inc=1, device_id={"tp": peer}, device_id_type=MESH)

    loads = [pltpu.make_async_copy(s, b.at[fs], load_sem.at[i]) for i, (s, b) in enumerate(zip(sources, bufs))]
    loads.append(pltpu.make_async_copy(tok_in, tok.at[tp], load_sem.at[7]))
    for c in loads:
        c.start()
    pl.semaphore_wait(barrier, expected)

    def cut(w):
        r = bufs[w].shape[1]
        a = max(16, (r * 13 // 16) // 16 * 16)
        return ((0, a), (a, r - a))

    def piece(w, k, block, way):
        start, size = cut(w)[k]
        ref = bufs[w].at[block, pl.ds(start, size)]
        return pltpu.make_async_remote_copy(
            src_ref=ref, dst_ref=ref,
            send_sem=send_sem.at[w, k, block, way], recv_sem=recv_sem.at[w, k, block],
            device_id={"fs": ways[way][1]}, device_id_type=MESH,
        )

    def arrive(w, k, block):
        piece(w, k, block, UP).wait_recv()

    def go(w, k, block, way, cond, sending):
        @pl.when(jnp.logical_and(cond, ways[way][0]))
        def _():
            c = piece(w, k, block, way)
            if sending:
                c.start()
            else:
                c.wait_send()

    yes = z >= 0

    def along_z(w, i, sending):
        half = (i + 1) // 2
        off = jnp.where(i % 2 == 1, -half, half)
        z0 = z + off
        valid = jnp.logical_and(z0 >= 0, z0 < nz)
        away = off != 0

        @pl.when(valid)
        def _():
            mine = z0 * nx + x

            def both(k, block):
                go(w, k, block, UP, z0 <= z, sending)
                go(w, k, block, DOWN, z0 >= z, sending)

            if sending:
                @pl.when(away)
                def _():
                    arrive(w, 0, mine)
            both(0, mine)
            go(w, 0, mine, RIGHT, yes, sending)
            go(w, 0, mine, LEFT, yes, sending)
            level = jnp.logical_not(away)

            @pl.loop(0, nx)
            def _(j):
                x0 = (x + j) % nx
                if sending:
                    @pl.when(jnp.logical_or(away, x != x0))
                    def _():
                        arrive(w, 1, z0 * nx + x0)
                go(w, 1, z0 * nx + x0, RIGHT, jnp.logical_and(level, x0 <= x), sending)
                go(w, 1, z0 * nx + x0, LEFT, jnp.logical_and(level, x0 >= x), sending)
                both(1, z0 * nx + x0)

    def along_x(w, i, sending):
        half = (i + 1) // 2
        z0 = z + jnp.where(i % 2 == 1, -half, half)

        @pl.when(jnp.logical_and(z0 >= 0, z0 < nz))
        def _():
            for dist in range(1, nx):
                for sign in (-1, 1):
                    x0 = x + sign * dist

                    @pl.when(jnp.logical_and(x0 >= 0, x0 < nx))
                    def _(sign=sign, x0=x0):
                        block = z0 * nx + x0
                        if sending:
                            arrive(w, 0, block)
                        go(w, 0, block, RIGHT if sign < 0 else LEFT, yes, sending)

    steps = 2 * nz - 1

    def step(w, i):
        @pl.when(i == 1)
        def _():
            row(w)

        @pl.when(i < steps)
        def _():
            along_z(w, i, True)
        along_x(w, i - 1, True)

    def pump(w, lo=1, hi=steps + 1):
        @pl.loop(lo, hi)
        def _(i):
            step(w, i)

    def during(w, lo, hi):
        def hook(j, total):
            first, last = j * (hi - lo) // total, (j + 1) * (hi - lo) // total

            @pl.loop(first, last)
            def _(i):
                step(w, lo + i)
        return hook

    def begin(w):
        loads[w].wait()
        for k in (1, 0):
            for way in (RIGHT, LEFT, UP, DOWN):
                go(w, k, fs, way, yes, True)

    def row(w):
        for dist in range(1, nx):
            for sign in (-1, 1):
                x0 = x + sign * dist

                @pl.when(jnp.logical_and(x0 >= 0, x0 < nx))
                def _(sign=sign, x0=x0):
                    block = z * nx + x0
                    arrive(w, 1, block)
                    for way in (RIGHT if sign < 0 else LEFT, UP, DOWN):
                        go(w, 1, block, way, yes, True)

    def to_owner(part, rs, send, recv, block):
        owner, k = block // per, block % per
        return owner, pltpu.make_async_remote_copy(
            src_ref=part.at[block], dst_ref=rs.at[tp, k],
            send_sem=send.at[block], recv_sem=recv.at[tp, k],
            device_id={"tp": owner}, device_id_type=MESH,
        )

    def from_peer(rs, recv, src, k):
        ref = rs.at[src, k]
        pltpu.make_async_remote_copy(
            src_ref=ref, dst_ref=ref, send_sem=p1_send.at[0], recv_sem=recv.at[src, k],
            device_id={"tp": src}, device_id_type=MESH,
        ).wait_recv()

    def spread(buf, send, recv):
        return [
            pltpu.make_async_remote_copy(
                src_ref=buf.at[tp], dst_ref=buf.at[tp], send_sem=send.at[r], recv_sem=recv.at[tp],
                device_id={"tp": peer}, device_id_type=MESH,
            )
            for r, peer in enumerate(peers)
        ]

    def collect(buf, send, recv):
        for peer in peers:
            pltpu.make_async_remote_copy(
                src_ref=buf.at[peer], dst_ref=buf.at[peer], send_sem=send.at[0], recv_sem=recv.at[peer],
                device_id={"tp": peer}, device_id_type=MESH,
            ).wait_recv()

    def norm(buf, gain, hook):
        high = 64

        @pl.loop(0, rows // high)
        def _(m):
            at = pl.ds(pl.multiple_of(m * high, high), high)
            total = jnp.zeros((high, 1), F32)
            for t in range(n_tp):
                v = buf[t, at, :].astype(F32)
                total = total + jnp.sum(v * v, axis=-1, keepdims=True)
            scale = lax.rsqrt(total / (n_tp * own) + EPS)
            for t in range(n_tp):
                cols = slice(t * own, (t + 1) * own)
                v = buf[t, at, :].astype(F32)
                normed[at, cols] = (v * scale * gain[:, cols]).astype(BF16)
            hook(m, rows // high)

    mt = 256 if rows % 256 == 0 else rows

    def project(w, dst, hook):
        n, r, c = bufs[w].shape
        mts = rows // mt
        pieces = -(-c // 256) * mts

        def column(index, start, size):
            @pl.loop(0, rows // mt)
            def _(m):
                at = pl.ds(pl.multiple_of(m * mt, mt), mt)
                weight = bufs[w][:, :, pl.ds(start, size)].reshape(n * r, size)
                dst[at, pl.ds(start, size)] = jnp.dot(
                    normed[at, :], weight, preferred_element_type=F32
                ).astype(BF16)
                hook(index * mts + m, pieces)
        tiles(c, 256, column)

    def out_block(w, act, part, rs, send, recv, block):
        @pl.loop(0, rows // mt)
        def _(m):
            at = pl.ds(pl.multiple_of(m * mt, mt), mt)
            part[block, at, :] = jnp.dot(
                act[at, :], bufs[w][block], preferred_element_type=F32
            ).astype(BF16)
        owner, c = to_owner(part, rs, send, recv, block)

        @pl.when(owner != tp)
        def _():
            c.start()

    def add_up(base, part, rs, recv, dst):
        for peer in peers:
            for k in range(per):
                from_peer(rs, recv, peer, k)
        high = 128

        @pl.loop(0, rows // high)
        def _(m):
            at = pl.ds(pl.multiple_of(m * high, high), high)
            for k in range(per):
                cols = slice(k * wide, (k + 1) * wide)
                total = part[tp * per + k, at, :].astype(F32)
                for peer in peers:
                    total = total + rs[peer, k, at, :].astype(F32)
                dst[at, cols] = (base[at, cols].astype(F32) + total).astype(BF16)

    begin(0)
    begin(1)
    loads[7].wait()
    tok_copies = spread(tok, tok_send, tok_recv)
    for c in tok_copies:
        c.start()
    pump(0)
    begin(2)
    pump(1)
    begin(3)
    collect(tok, tok_send, tok_recv)
    norm(tok, mix_gain, during(2, 1, steps + 1))
    begin(4)
    middle = (steps + 2) // 2
    project(0, outer, during(3, 1, middle))
    project(1, inner, during(3, middle, steps + 1))
    begin(5)
    project(2, signal, during(4, 1, 3))

    def mixer(index, start, size):
        cols = pl.ds(start, size)
        taps = [mix_taps[j:j + 1, cols] for j in range(3)]
        v = inner[:, cols].astype(F32) * signal[:, cols].astype(F32)
        outer[:, cols] = (outer[:, cols].astype(F32) * causal(v, taps, mix_bias[:, cols])).astype(BF16)
    tiles(outer.shape[1], 128, mixer)

    @pl.loop(0, n_fs)
    def _(block):
        out_block(3, outer, part1, rs1, p1_send, p1_recv, block)
    pump(4, 3, middle + 2)
    add_up(tok.at[tp], part1, rs1, p1_recv, state.at[tp])
    st_copies = spread(state, st_send, st_recv)
    for c in st_copies:
        c.start()
    pump(4, middle + 2)
    begin(6)
    pump(5, 1, middle)
    collect(state, st_send, st_recv)
    norm(state, ffn_gain, during(5, middle, middle + 2))
    project(4, gate, during(5, middle + 2, steps + 1))
    project(5, value, during(6, 1, middle))

    def feed(index, start, size):
        cols = pl.ds(start, size)
        g = causal(gate[:, cols].astype(F32), [ffn_taps[j:j + 1, cols] for j in range(3)], ffn_bias[0:1, cols])
        v = causal(value[:, cols].astype(F32), [ffn_taps[j:j + 1, cols] for j in range(3, 6)], ffn_bias[1:2, cols])
        gate[:, cols] = (g / (1.0 + jnp.exp(-g)) * v).astype(BF16)
        during(6, middle, middle + 1)(index, -(-gate.shape[1] // 128))
    tiles(gate.shape[1], 128, feed)
    fed_from = middle + 1

    @pl.loop(0, steps + 1)
    def _(i):
        def block_out(block):
            out_block(6, gate, part2, rs2, p2_send, p2_recv, block)

        half = (i + 1) // 2
        z0 = z + jnp.where(i % 2 == 1, -half, half)
        before = i // 2
        z1 = z + jnp.where(i % 2 == 0, -before, before)

        @pl.when(jnp.logical_and(i >= fed_from, i < steps))
        def _():
            along_z(6, i, True)

        @pl.when(i >= fed_from)
        def _():
            along_x(6, i - 1, True)

        @pl.loop(0, nx)
        def _(j):
            z_of = jnp.where(j == 0, z0, z1)
            good = jnp.logical_and(z_of >= 0, z_of < nz)
            good = jnp.logical_and(good, jnp.where(j == 0, i < steps, i >= 1))

            @pl.when(good)
            def _():
                block_out(z_of * nx + (x + j) % nx)

    add_up(state.at[tp], part2, rs2, p2_recv, out)

    for c in tok_copies + st_copies:
        c.wait_send()
    for part, rs, send, recv in ((part1, rs1, p1_send, p1_recv), (part2, rs2, p2_send, p2_recv)):
        @pl.loop(0, n_fs)
        def _(block):
            owner, c = to_owner(part, rs, send, recv, block)

            @pl.when(owner != tp)
            def _():
                c.wait_send()
    for w in range(7):
        @pl.loop(0, steps)
        def _(i):
            along_z(w, i, False)
            along_x(w, i, False)


def solution(mesh):
    n_fs, n_tp = mesh.shape["fs"], mesh.shape["tp"]

    def on_device(
        tokens, mix_gain, outer_gate, inner_gate, signal_in, mix_taps, mix_bias, mix_out,
        ffn_gain, up_gate, up_value, ffn_taps, ffn_bias, down_proj,
    ):
        rows, own = tokens.shape
        weights = (outer_gate, inner_gate, signal_in, mix_out, up_gate, up_value, down_proj)
        chan, hidden = outer_gate.shape[1], up_gate.shape[1]
        wide = mix_out.shape[1]
        model = own * n_tp
        hbm = pl.BlockSpec(memory_space=pl.ANY)
        vmem = pl.BlockSpec(memory_space=pltpu.VMEM)
        dma = pltpu.SemaphoreType.DMA
        per = n_fs // n_tp
        return pl.pallas_call(
            functools.partial(kernel, n_fs, n_tp),
            out_shape=jax.ShapeDtypeStruct(tokens.shape, BF16),
            in_specs=[hbm] * 8 + [vmem] * 6,
            out_specs=vmem,
            scratch_shapes=[pltpu.VMEM((n_fs, *w.shape), BF16) for w in weights]
            + [
                pltpu.VMEM((n_tp, rows, own), BF16),
                pltpu.VMEM((rows, model), BF16),
                pltpu.VMEM((n_tp, rows, own), BF16),
                pltpu.VMEM((rows, chan), BF16),
                pltpu.VMEM((rows, chan), BF16),
                pltpu.VMEM((rows, chan), BF16),
                pltpu.VMEM((rows, hidden), BF16),
                pltpu.VMEM((rows, hidden), BF16),
                pltpu.VMEM((n_fs, rows, wide), BF16),
                pltpu.VMEM((n_tp, per, rows, wide), BF16),
                pltpu.VMEM((n_fs, rows, wide), BF16),
                pltpu.VMEM((n_tp, per, rows, wide), BF16),
                dma((8,)),
                dma((7, 2, n_fs, 4)),
                dma((7, 2, n_fs)),
                dma((n_tp,)), dma((n_tp,)),
                dma((n_tp,)), dma((n_tp,)),
                dma((n_fs,)), dma((n_tp, per)),
                dma((n_fs,)), dma((n_tp, per)),
            ],
            compiler_params=pltpu.CompilerParams(
                collective_id=0, has_side_effects=True, vmem_limit_bytes=67043328
            ),
        )(
            tokens, *weights, mix_gain[None], ffn_gain[None], mix_taps, mix_bias[None],
            ffn_taps.reshape(6, hidden), ffn_bias,
        )

    return jax.shard_map(
        on_device,
        mesh=mesh,
        in_specs=(
            P("fs", "tp"), P(), P("fs", "tp"), P("fs", "tp"), P("fs", "tp"), P(None, "tp"), P("tp"),
            P("tp", "fs"), P(), P("fs", "tp"), P("fs", "tp"), P(None, None, "tp"), P(None, "tp"),
            P("tp", "fs"),
        ),
        out_specs=P("fs", "tp"),
        check_vma=False,
    )
```

profile of v0, /device:TPU:3, one launch (start us, length us, event | category | flops | bytes accessed | tf_op | source)
XLA Modules:
  0.0 325.8 jit_solution(10300091555649495810)
XLA Ops:
  0.0 0.8 copy.16
  0.8 0.6 reshape.3.ffn_taps
  1.4 322.3 %shard_map.136 = bf16[768,512]{1,0:T(8,128)(2,1)} custom-call(bf16[768,512]{1,0:T(8,128)(2,1)} %tok_in.1, bf16[256,512]{1,0:T(8,128)(2,1)} %og.1, bf16[256,512]{1,0:T(8,128)(2,1)} %ig.1, bf16[256,512]{1,0:T(8,128)(2,1)} %si.1, bf16[512,256]{1,0:T(8,128)(2,1)} %mo.1, bf16[256,1408]{1,0:T(8,128)(2,1)} %ug.1, bf16[256,1408]{1,0:T(8,128)(2,1)} %uv.1, ...), custom_call_target="tpu_custom_call" | custom-call | tf_op jit(solution)/shard_map/pallas_call | solution.py:416
  323.7 2.1 copy.18
where the time goes:
time: 328 us; the launch traced here: 326 us
  Pallas kernels  322 us (98%)
  local copies, waits for them, and re-layouts  3.47 us (1%)
    pallas_call x1, Pallas kernels, on_device(): pl.pallas_call(functools.partial(kernel, n_fs, n_tp), out_shape=jax.Shape...  322 us

commit v1 on v0

v1 whole, which is shorter than its diff:
```python
import functools

import jax
import jax.numpy as jnp
from jax import lax
from jax.experimental import pallas as pl
from jax.experimental.pallas import tpu as pltpu
from jax.sharding import PartitionSpec as P

EPS = 1e-06
F32, BF16 = jnp.float32, jnp.bfloat16
MESH = pl.DeviceIdType.MESH
UP, DOWN, RIGHT, LEFT = range(4)


def grid_of(n_fs):
    nx = 1
    while nx * nx * 4 <= n_fs:
        nx *= 2
    return n_fs // nx, nx


def tiles(extent, width, body):
    whole = extent // width
    if whole:
        @pl.loop(0, whole)
        def _(i):
            body(i, pl.multiple_of(i * width, width), width)
    if extent % width:
        body(whole, whole * width, extent % width)


def causal(v, taps, bias):
    row = lax.broadcasted_iota(jnp.int32, v.shape, 0)
    first = jnp.where(row < 1, 0.0, pltpu.roll(v, 1, axis=0))
    second = jnp.where(row < 2, 0.0, pltpu.roll(v, 2, axis=0))
    return taps[2] * v + taps[1] * first + taps[0] * second + bias


def kernel(
    n_fs, n_tp, tok_in, og, ig, si, mo, ug, uv, dp,
    mix_gain, ffn_gain, mix_taps, mix_bias, ffn_taps, ffn_bias,
    out,
    w0, w1, w2, w3, f0, f1, f2,
    tok, normed, state, outer, inner, signal, gate, value,
    part1, sib1, rs1, part2, sib2, rs2,
    load_sem, send_sem, recv_sem, fsend, ffar, frecv,
    tok_sib, tok_y, tok_recv, st_sib, st_y, st_z, st_recv,
    s1_send, s1_recv, p1_send, p1_recv, s2_send, s2_recv, p2_send, p2_recv,
):
    nz, nx = grid_of(n_fs)
    fs, tp = lax.axis_index("fs"), lax.axis_index("tp")
    z, x = fs // nx, fs % nx
    ny = n_tp // 2
    y, core = tp // 2, tp % 2
    mate = tp + 1 - 2 * core
    pair = (z + 1 - 2 * (z % 2)) * nx + x
    bufs = (w0, w1, w2, w3)
    fbufs = (f0, f1, f2)
    fowns = (ug, uv, dp)
    rows, own = tok.shape[2], tok.shape[3]
    per = n_fs // n_tp
    wide = part1.shape[3]
    hidden = ug.shape[1]
    big = f0.shape[2]
    small = hidden - big
    outside = jnp.logical_or(z == 0, z == nz - 1)
    inside = jnp.logical_not(outside)

    ways = (
        (z < nz - 1, fs + nx),
        (z > 0, fs - nx),
        (x < nx - 1, fs + 1),
        (x > 0, fs - 1),
    )
    barrier = pltpu.get_barrier_semaphore()
    expected = n_tp - 1 + nz - 1 + ny - 1
    for there, peer in ways[2:]:
        expected = expected + jnp.where(there, 1, 0)

        @pl.when(there)
        def _(peer=peer):
            pl.semaphore_signal(barrier, inc=1, device_id={"fs": peer}, device_id_type=MESH)
    for r in range(1, nz):
        pl.semaphore_signal(barrier, inc=1, device_id={"fs": (z + r) % nz * nx + x}, device_id_type=MESH)
    for r in range(1, n_tp):
        pl.semaphore_signal(barrier, inc=1, device_id={"tp": (tp + r) % n_tp}, device_id_type=MESH)
    ypeers = [(y + r) % ny for r in range(1, ny)]
    for yy in ypeers:
        pl.semaphore_signal(
            barrier, inc=1, device_id={"fs": pair, "tp": yy * 2 + core}, device_id_type=MESH
        )

    loads = [pltpu.make_async_copy(a, b.at[fs], load_sem.at[i]) for i, (a, b) in enumerate(zip((og, ig, si, mo), bufs))]
    loads.append(pltpu.make_async_copy(tok_in, tok.at[0, tp], load_sem.at[4]))
    for c in loads:
        c.start()

    def span(p):
        return (0, big) if p else (big, small)

    def held(w, p, block):
        size = span(p)[1]
        return fbufs[w].at[block, pl.ds(0, size)] if w == 2 else fbufs[w].at[block, :, pl.ds(0, size)]

    def source(w, p):
        start, size = span(p)
        return fowns[w].at[pl.ds(start, size)] if w == 2 else fowns[w].at[:, pl.ds(start, size)]

    def each_part(body):
        @pl.when(outside)
        def _():
            body(0)

        @pl.when(inside)
        def _():
            body(1)

    def own_f(w, starting):
        def body(p):
            c = pltpu.make_async_copy(source(w, p), held(w, p, fs), load_sem.at[5 + w])
            if starting:
                c.start()
            else:
                c.wait()
        each_part(body)

    for w in range(3):
        own_f(w, True)
    if small < big:
        @pl.when(outside)
        def _():
            for w in range(2):
                fbufs[w][:, :, small:big] = jnp.zeros((n_fs, f0.shape[1], big - small), BF16)
            f2[:, small:big, :] = jnp.zeros((n_fs, big - small, wide), BF16)
    pl.semaphore_wait(barrier, expected)

    def cut(w):
        r = bufs[w].shape[1]
        a = max(16, (r * 13 // 16) // 16 * 16)
        return ((0, a), (a, r - a))

    def piece(w, k, block, way):
        start, size = cut(w)[k]
        ref = bufs[w].at[block, pl.ds(start, size)]
        return pltpu.make_async_remote_copy(
            src_ref=ref, dst_ref=ref,
            send_sem=send_sem.at[w, k, block, way], recv_sem=recv_sem.at[w, k, block],
            device_id={"fs": ways[way][1]}, device_id_type=MESH,
        )

    def arrive(w, k, block):
        piece(w, k, block, UP).wait_recv()

    def run(cond, c, sending):
        @pl.when(cond)
        def _():
            if sending:
                c.start()
            else:
                c.wait_send()

    def go(w, k, block, way, cond, sending):
        run(jnp.logical_and(cond, ways[way][0]), piece(w, k, block, way), sending)

    yes = z >= 0
    steps = 2 * nz - 1

    def layer(i):
        half = (i + 1) // 2
        z0 = z + jnp.where(i % 2 == 1, -half, half)
        return z0, jnp.logical_and(z0 >= 0, z0 < nz)

    def along_z(w, i, sending):
        z0, valid = layer(i)
        away = z0 != z

        @pl.when(valid)
        def _():
            mine = z0 * nx + x

            def both(k, block):
                go(w, k, block, UP, z0 <= z, sending)
                go(w, k, block, DOWN, z0 >= z, sending)

            if sending:
                @pl.when(away)
                def _():
                    arrive(w, 0, mine)
            both(0, mine)
            go(w, 0, mine, RIGHT, yes, sending)
            go(w, 0, mine, LEFT, yes, sending)
            level = jnp.logical_not(away)

            @pl.loop(0, nx)
            def _(j):
                x0 = (x + j) % nx
                if sending:
                    @pl.when(jnp.logical_or(away, x != x0))
                    def _():
                        arrive(w, 1, z0 * nx + x0)
                go(w, 1, z0 * nx + x0, RIGHT, jnp.logical_and(level, x0 <= x), sending)
                go(w, 1, z0 * nx + x0, LEFT, jnp.logical_and(level, x0 >= x), sending)
                both(1, z0 * nx + x0)

    def sides(body):
        for dist in range(1, nx):
            for sign in (-1, 1):
                x0 = x + sign * dist

                @pl.when(jnp.logical_and(x0 >= 0, x0 < nx))
                def _(sign=sign, x0=x0):
                    body(x0, RIGHT if sign < 0 else LEFT)

    def along_x(w, i, sending):
        z0, valid = layer(i)

        @pl.when(valid)
        def _():
            def body(x0, way):
                if sending:
                    arrive(w, 0, z0 * nx + x0)
                go(w, 0, z0 * nx + x0, way, yes, sending)
            sides(body)

    def step(w, i):
        @pl.when(i == 1)
        def _():
            row(w)

        @pl.when(i < steps)
        def _():
            along_z(w, i, True)
        along_x(w, i - 1, True)

    def pump(w, lo=1, hi=steps + 1):
        @pl.loop(lo, hi)
        def _(i):
            step(w, i)

    def spaced(move, lo, hi):
        def hook(j, total):
            first, last = j * (hi - lo) // total, (j + 1) * (hi - lo) // total

            @pl.loop(first, last)
            def _(i):
                move(lo + i)
        return hook

    def during(w, lo, hi):
        return spaced(lambda i: step(w, i), lo, hi)

    def begin(w):
        loads[w].wait()
        for k in (1, 0):
            for way in (RIGHT, LEFT, UP, DOWN):
                go(w, k, fs, way, yes, True)

    def row(w):
        def body(x0, way):
            block = z * nx + x0
            arrive(w, 1, block)
            for to in (way, UP, DOWN):
                go(w, 1, block, to, yes, True)
        sides(body)

    def fcopy(w, p, block, src, target, sem):
        return pltpu.make_async_remote_copy(
            src_ref=src, dst_ref=held(w, p, block), send_sem=sem, recv_sem=frecv.at[w, block],
            device_id={"fs": target}, device_id_type=MESH,
        )

    def fgo(w, p, block, src, way, cond, sending):
        there, target = ways[way]
        run(jnp.logical_and(cond, there), fcopy(w, p, block, src, target, fsend.at[w, block, way]), sending)

    def farrive(w, p, block):
        fcopy(w, p, block, held(w, p, block), fs, fsend.at[w, block, 0]).wait_recv()

    up_in = jnp.logical_and(z + 1 >= 1, z + 1 <= nz - 2)
    down_in = jnp.logical_and(z - 1 >= 1, z - 1 <= nz - 2)

    def begin_fx(w, sending=True):
        for p, cond in ((0, outside), (1, inside)):
            for way in (RIGHT, LEFT):
                fgo(w, p, fs, source(w, p), way, cond, sending)

    def begin_fz(w, sending=True):
        fgo(w, 1, fs, source(w, 1), UP, up_in, sending)
        fgo(w, 1, fs, source(w, 1), DOWN, down_in, sending)
        for e, end in enumerate((0, nz - 1)):
            run(z != end, fcopy(w, 0, fs, source(w, 0), end * nx + x, ffar.at[w, e]), sending)

    def frelay(w, i, sending=True):
        z0, valid = layer(i)
        block = z0 * nx + x

        @pl.when(jnp.logical_and(valid, z0 != z))
        def _():
            def body(p):
                ref = held(w, p, block)
                if sending:
                    farrive(w, p, block)
                if p:
                    fgo(w, p, block, ref, UP, jnp.logical_and(z0 < z, up_in), sending)
                    fgo(w, p, block, ref, DOWN, jnp.logical_and(z0 > z, down_in), sending)
                fgo(w, p, block, ref, RIGHT, yes, sending)
                fgo(w, p, block, ref, LEFT, yes, sending)
            each_part(body)

    def fside(w, i, sending=True):
        z0, valid = layer(i)

        @pl.when(valid)
        def _():
            def part(p):
                def body(x0, way):
                    block = z0 * nx + x0
                    if sending:
                        farrive(w, p, block)
                    fgo(w, p, block, held(w, p, block), way, yes, sending)
                sides(body)
            each_part(part)

    def frelays(w, lo, hi):
        @pl.loop(lo, hi)
        def _(i):
            frelay(w, i)

    def fduring(w, lo, hi):
        return spaced(lambda i: frelay(w, i), lo, hi)

    def fsides(w):
        @pl.loop(0, steps)
        def _(i):
            fside(w, i)

    def send(ref, send, recv, to):
        return pltpu.make_async_remote_copy(
            src_ref=ref[0], dst_ref=ref[1], send_sem=send, recv_sem=recv, device_id=to, device_id_type=MESH
        )

    def got(ref, recv):
        send((ref, ref), st_z.at[0], recv, {"tp": mate}).wait_recv()

    def to_mate(buf, s, t, sib, recv):
        return send((buf.at[s, t], buf.at[s, t]), sib.at[s, t], recv.at[s, t], {"tp": mate})

    def to_ys(buf, s, ysend, recv):
        ref = buf.at[s, tp]
        return [
            send((ref, ref), ysend.at[s, r], recv.at[s, tp], {"tp": yy * 2 + core})
            for r, yy in enumerate(ypeers)
        ]

    def ag_out(buf, s, sib, ysend, recv):
        for c in to_ys(buf, s, ysend, recv):
            c.start()
        to_mate(buf, s, tp, sib, recv).start()

    def ag_relay(buf, s, sib, recv):
        for yy in ypeers:
            t = yy * 2 + core
            got(buf.at[s, t], recv.at[s, t])
            to_mate(buf, s, t, sib, recv).start()

    def ag_done(buf, s, recv):
        for yy in range(ny):
            t = yy * 2 + 1 - core
            got(buf.at[s, t], recv.at[s, t])

    def ag_sent(buf, s, sib, ysend, recv):
        for c in to_ys(buf, s, ysend, recv):
            c.wait_send()
        for yy in range(ny):
            to_mate(buf, s, yy * 2 + core, sib, recv).wait_send()

    def norm(buf, s, gain, hook):
        high = 64

        @pl.loop(0, rows // high)
        def _(m):
            at = pl.ds(pl.multiple_of(m * high, high), high)
            total = jnp.zeros((high, 1), F32)
            for t in range(n_tp):
                v = buf[s, t, at, :].astype(F32)
                total = total + jnp.sum(v * v, axis=-1, keepdims=True)
            scale = lax.rsqrt(total / (n_tp * own) + EPS)
            for t in range(n_tp):
                cols = slice(t * own, (t + 1) * own)
                v = buf[s, t, at, :].astype(F32)
                normed[s, at, cols] = (v * scale * gain[:, cols]).astype(BF16)
            hook(m, rows // high)

    mt = 256 if rows % 256 == 0 else rows

    def none(j, total):
        pass

    def project(weights, s, dst, hook):
        n, r, c = weights.shape
        mts = rows // mt
        pieces = -(-c // 256) * mts

        def column(index, start, size):
            @pl.loop(0, mts)
            def _(m):
                at = pl.ds(pl.multiple_of(m * mt, mt), mt)
                weight = weights[:, :, pl.ds(start, size)].reshape(n * r, size)
                dst[s, at, pl.ds(start, size)] = jnp.dot(
                    normed[s, at, :], weight, preferred_element_type=F32
                ).astype(BF16)
                hook(index * mts + m, pieces)
        tiles(c, 256, column)

    def owner(block):
        t = block // per
        return t // 2, t % 2, block % per

    def out_block(weights, act, seqs, part, sib, ssend, srecv, block):
        for s in range(seqs):
            @pl.loop(0, rows // mt)
            def _(m):
                at = pl.ds(pl.multiple_of(m * mt, mt), mt)
                part[block, s, at, :] = jnp.dot(
                    act[s, at, :], weights[block], preferred_element_type=F32
                ).astype(BF16)
        yo, co, k = owner(block)
        run(co != core, mate_copy(part, sib, ssend, srecv, block), True)

    def mate_copy(part, sib, ssend, srecv, block):
        yo, co, k = owner(block)
        slot = yo * per + k
        return send((part.at[block], sib.at[slot]), ssend.at[slot], srecv.at[slot], {"tp": mate})

    def home_copy(part, s, rs, psend, precv, block, rel):
        yo, co, k = owner(block)
        to = {"tp": yo * 2 + core} if rel == 0 else {"fs": pair, "tp": yo * 2 + core}
        return send((part.at[block, s], rs.at[rel, y, k]), psend.at[rel, yo, k], precv.at[rel, y, k], to)

    def combine(seqs, part, sib, rs, srecv, psend, precv, block):
        yo, co, k = owner(block)
        slot = yo * per + k

        @pl.when(co == core)
        def _():
            got(sib.at[slot], srecv.at[slot])
            high = 128
            for s in reversed(range(seqs)):
                @pl.loop(0, rows // high)
                def _(m):
                    at = pl.ds(pl.multiple_of(m * high, high), high)
                    part[block, s, at, :] = (
                        part[block, s, at, :].astype(F32) + sib[slot, s, at, :].astype(F32)
                    ).astype(BF16)
                run(yes if s else yo != y, home_copy(part, s, rs, psend, precv, block, s), True)

    def sent_home(seqs, part, sib, rs, ssend, srecv, psend, precv):
        @pl.loop(0, n_fs)
        def _(block):
            yo, co, k = owner(block)
            run(co != core, mate_copy(part, sib, ssend, srecv, block), False)
            for s in range(seqs):
                run(
                    co == core if s else jnp.logical_and(co == core, yo != y),
                    home_copy(part, s, rs, psend, precv, block, s), False,
                )

    def add_up(base, seqs, part, rs, precv, dst):
        for rel in range(seqs):
            for yy in (ypeers if rel == 0 else ypeers + [y]):
                for k in range(per):
                    got(rs.at[rel, yy, k], precv.at[rel, yy, k])
        high = 128

        @pl.loop(0, rows // high)
        def _(m):
            at = pl.ds(pl.multiple_of(m * high, high), high)
            for k in range(per):
                cols = slice(k * wide, (k + 1) * wide)
                total = part[tp * per + k, 0, at, :].astype(F32)
                for rel in range(seqs):
                    for yy in (ypeers if rel == 0 else ypeers + [y]):
                        total = total + rs[rel, yy, k, at, :].astype(F32)
                dst[at, cols] = (base[at, cols].astype(F32) + total).astype(BF16)

    def sweep(move, form, merge):
        @pl.loop(0, steps + 2)
        def _(i):
            move(i)

            def blocks(i, body):
                @pl.loop(0, nx)
                def _(j):
                    i0 = jnp.where(j == 0, i, i - 1)
                    z0, good = layer(i0)
                    good = jnp.logical_and(good, jnp.logical_and(i0 >= 0, i0 < steps))

                    @pl.when(good)
                    def _():
                        body(z0 * nx + (x + j) % nx)
            blocks(i, form)
            blocks(i - 1, merge)

    tok_sems = (tok_sib, tok_y, tok_recv)
    st_sems = (st_sib, st_y, st_recv)

    begin(0)
    begin(1)
    loads[4].wait()
    ag_out(tok, 0, *tok_sems)
    pump(0)
    begin(2)
    ag_relay(tok, 0, tok_sib, tok_recv)
    pump(1, 1, 3)
    ag_done(tok, 0, tok_recv)
    norm(tok, 0, mix_gain, during(1, 3, 6))
    project(w0, 0, outer, during(1, 6, steps + 1))
    begin(3)
    project(w1, 0, inner, during(2, 1, 4))
    pump(2, 4)
    begin_fx(0)
    begin_fz(0)
    project(w2, 0, signal, during(3, 1, 3))

    def mixer(index, start, size):
        cols = pl.ds(start, size)
        taps = [mix_taps[j:j + 1, cols] for j in range(3)]
        v = inner[0, :, cols].astype(F32) * signal[0, :, cols].astype(F32)
        outer[0, :, cols] = (outer[0, :, cols].astype(F32) * causal(v, taps, mix_bias[:, cols])).astype(BF16)
    tiles(outer.shape[2], 128, mixer)

    def move1(i):
        @pl.when(jnp.logical_and(i >= 3, i <= steps))
        def _():
            step(3, i)
    sweep(
        move1,
        lambda b: out_block(w3, outer, 1, part1, sib1, s1_send, s1_recv, b),
        lambda b: combine(1, part1, sib1, rs1, s1_recv, p1_send, p1_recv, b),
    )
    begin_fx(1)
    frelays(0, 1, 3)
    add_up(tok.at[0, tp], 1, part1, rs1, p1_recv, state.at[0, tp])
    to_pair = send((state.at[0, tp], state.at[1, tp]), st_z.at[0], st_recv.at[1, tp], {"fs": pair})
    to_pair.start()
    ag_out(state, 0, *st_sems)
    begin_fz(1)
    frelays(0, 3, steps)
    ag_relay(state, 0, st_sib, st_recv)
    frelays(1, 1, 3)
    got(state.at[1, tp], st_recv.at[1, tp])
    ag_out(state, 1, *st_sems)
    begin_fx(2)
    begin_fz(2)
    ag_done(state, 0, st_recv)
    norm(state, 0, ffn_gain, none)
    for w in range(3):
        own_f(w, False)
    fsides(0)
    project(f0, 0, gate, fduring(1, 3, 5))
    ag_relay(state, 1, st_sib, st_recv)
    ag_done(state, 1, st_recv)
    norm(state, 1, ffn_gain, fduring(1, 5, steps))
    project(f0, 1, gate, fduring(2, 1, 3))
    fsides(1)
    project(f1, 0, value, none)
    project(f1, 1, value, none)
    shift = jnp.where(outside, big, 0)

    @pl.loop(0, jnp.where(outside, small, big) // 128)
    def _(i):
        cols = pl.ds(pl.multiple_of(i * 128, 128), 128)
        at = pl.ds(pl.multiple_of(shift + i * 128, 128), 128)
        for s in range(2):
            g = causal(gate[s, :, cols].astype(F32), [ffn_taps[j:j + 1, at] for j in range(3)], ffn_bias[0:1, at])
            v = causal(value[s, :, cols].astype(F32), [ffn_taps[j:j + 1, at] for j in range(3, 6)], ffn_bias[1:2, at])
            gate[s, :, cols] = (g / (1.0 + jnp.exp(-g)) * v).astype(BF16)

    def move2(i):
        @pl.when(jnp.logical_and(i >= 3, i < steps))
        def _():
            frelay(2, i)

        @pl.when(jnp.logical_and(i >= 1, i <= steps))
        def _():
            fside(2, i - 1)
    sweep(
        move2,
        lambda b: out_block(f2, gate, 2, part2, sib2, s2_send, s2_recv, b),
        lambda b: combine(2, part2, sib2, rs2, s2_recv, p2_send, p2_recv, b),
    )
    add_up(state.at[0, tp], 2, part2, rs2, p2_recv, out)

    to_pair.wait_send()
    ag_sent(tok, 0, *tok_sems)
    ag_sent(state, 0, *st_sems)
    ag_sent(state, 1, *st_sems)
    sent_home(1, part1, sib1, rs1, s1_send, s1_recv, p1_send, p1_recv)
    sent_home(2, part2, sib2, rs2, s2_send, s2_recv, p2_send, p2_recv)
    for w in range(4):
        @pl.loop(0, steps)
        def _(i):
            along_z(w, i, False)
            along_x(w, i, False)
    for w in range(3):
        begin_fx(w, False)
        begin_fz(w, False)

        @pl.loop(0, steps)
        def _(i):
            frelay(w, i, False)
            fside(w, i, False)


def solution(mesh):
    n_fs, n_tp = mesh.shape["fs"], mesh.shape["tp"]

    def on_device(
        tokens, mix_gain, outer_gate, inner_gate, signal_in, mix_taps, mix_bias, mix_out,
        ffn_gain, up_gate, up_value, ffn_taps, ffn_bias, down_proj,
    ):
        rows, own = tokens.shape
        ffn_taps = ffn_taps.reshape(6, -1)
        spare = -up_gate.shape[1] % 128
        if spare:
            up_gate, up_value, ffn_taps, ffn_bias = (
                jnp.pad(a, ((0, 0), (0, spare))) for a in (up_gate, up_value, ffn_taps, ffn_bias)
            )
            down_proj = jnp.pad(down_proj, ((0, spare), (0, 0)))
        weights = (outer_gate, inner_gate, signal_in, mix_out)
        chan, hidden = outer_gate.shape[1], up_gate.shape[1]
        depth, wide = outer_gate.shape[0], mix_out.shape[1]
        big = hidden - hidden // 256 * 128
        model = own * n_tp
        hbm = pl.BlockSpec(memory_space=pl.ANY)
        vmem = pl.BlockSpec(memory_space=pltpu.VMEM)
        dma = pltpu.SemaphoreType.DMA
        per, ny = n_fs // n_tp, n_tp // 2
        return pl.pallas_call(
            functools.partial(kernel, n_fs, n_tp),
            out_shape=jax.ShapeDtypeStruct(tokens.shape, BF16),
            in_specs=[hbm] * 8 + [vmem] * 6,
            out_specs=vmem,
            scratch_shapes=[pltpu.VMEM((n_fs, *w.shape), BF16) for w in weights]
            + [
                pltpu.VMEM((n_fs, depth, big), BF16),
                pltpu.VMEM((n_fs, depth, big), BF16),
                pltpu.VMEM((n_fs, big, wide), BF16),
                pltpu.VMEM((1, n_tp, rows, own), BF16),
                pltpu.VMEM((2, rows, model), BF16),
                pltpu.VMEM((2, n_tp, rows, own), BF16),
                pltpu.VMEM((1, rows, chan), BF16),
                pltpu.VMEM((1, rows, chan), BF16),
                pltpu.VMEM((1, rows, chan), BF16),
                pltpu.VMEM((2, rows, big), BF16),
                pltpu.VMEM((2, rows, big), BF16),
                pltpu.VMEM((n_fs, 1, rows, wide), BF16),
                pltpu.VMEM((ny * per, 1, rows, wide), BF16),
                pltpu.VMEM((1, ny, per, rows, wide), BF16),
                pltpu.VMEM((n_fs, 2, rows, wide), BF16),
                pltpu.VMEM((ny * per, 2, rows, wide), BF16),
                pltpu.VMEM((2, ny, per, rows, wide), BF16),
                dma((8,)),
                dma((4, 2, n_fs, 4)),
                dma((4, 2, n_fs)),
                dma((3, n_fs, 4)),
                dma((3, 2)),
                dma((3, n_fs)),
                dma((1, n_tp)), dma((1, ny)), dma((1, n_tp)),
                dma((2, n_tp)), dma((2, ny)), dma((1,)), dma((2, n_tp)),
                dma((ny * per,)), dma((ny * per,)), dma((1, ny, per)), dma((1, ny, per)),
                dma((ny * per,)), dma((ny * per,)), dma((2, ny, per)), dma((2, ny, per)),
            ],
            compiler_params=pltpu.CompilerParams(
                collective_id=0, has_side_effects=True, vmem_limit_bytes=67043328
            ),
        )(
            tokens, *weights, up_gate, up_value, down_proj, mix_gain[None], ffn_gain[None], mix_taps, mix_bias[None],
            ffn_taps, ffn_bias,
        )

    return jax.shard_map(
        on_device,
        mesh=mesh,
        in_specs=(
            P("fs", "tp"), P(), P("fs", "tp"), P("fs", "tp"), P("fs", "tp"), P(None, "tp"), P("tp"),
            P("tp", "fs"), P(), P("fs", "tp"), P("fs", "tp"), P(None, None, "tp"), P(None, "tp"),
            P("tp", "fs"),
        ),
        out_specs=P("fs", "tp"),
        check_vma=False,
    )
```

time: 328 us -> 289 us (0.88)
  Pallas kernels: 322 us -> 283 us
    pallas_call x1, Pallas kernels: 322 us -> 283 us  [on_device(): pl.pallas_call(functools.partial(kernel, n_fs, n_tp), out_shape=jax.Shape...]
where the time goes in v1:
time: 289 us; the launch traced here: 287 us
  Pallas kernels  283 us (98%)
  local copies, waits for them, and re-layouts  3.47 us (1%)
    pallas_call x1, Pallas kernels, on_device(): pl.pallas_call(functools.partial(kernel, n_fs, n_tp), out_shape=jax.Shape...  283 us

profile of v1, /device:TPU:3, one launch (start us, length us, event | category | flops | bytes accessed | tf_op | source)
XLA Modules:
  0.0 286.6 jit_solution(5588355269867323104)
XLA Ops:
  0.0 0.8 copy.16
  0.8 0.6 reshape.3.ffn_taps
  1.4 283.1 %shard_map.136 = bf16[768,512]{1,0:T(8,128)(2,1)} custom-call(bf16[768,512]{1,0:T(8,128)(2,1)} %tok_in.1, bf16[256,512]{1,0:T(8,128)(2,1)} %og.1, bf16[256,512]{1,0:T(8,128)(2,1)} %ig.1, bf16[256,512]{1,0:T(8,128)(2,1)} %si.1, bf16[512,256]{1,0:T(8,128)(2,1)} %mo.1, bf16[256,1408]{1,0:T(8,128)(2,1)} %ug.1, bf16[256,1408]{1,0:T(8,128)(2,1)} %uv.1, ...), custom_call_target="tpu_custom_call" | custom-call | tf_op jit(solution)/shard_map/pallas_call | solution.py:640
  284.5 2.1 copy.18

commit v2 on v1

--- a/solution.py
+++ b/solution.py
@@ -43,10 +43,10 @@
     out,
     w0, w1, w2, w3, f0, f1, f2,
     tok, normed, state, outer, inner, signal, gate, value,
-    part1, sib1, rs1, part2, sib2, rs2,
+    part1, sib1, rs1, part2, sib2, rs2, far2,
     load_sem, send_sem, recv_sem, fsend, ffar, frecv,
     tok_sib, tok_y, tok_recv, st_sib, st_y, st_z, st_recv,
-    s1_send, s1_recv, p1_send, p1_recv, s2_send, s2_recv, p2_send, p2_recv,
+    s1_send, s1_recv, p1_send, p1_recv, s2_send, s2_recv, p2_send, p2_recv, far_send, far_recv,
 ):
     nz, nx = grid_of(n_fs)
     fs, tp = lax.axis_index("fs"), lax.axis_index("tp")
@@ -164,44 +164,38 @@
         run(jnp.logical_and(cond, ways[way][0]), piece(w, k, block, way), sending)
 
     yes = z >= 0
-    steps = 2 * nz - 1
+    steps = nz
+    near = jnp.minimum(z, nz - 1 - z)
 
     def layer(i):
-        half = (i + 1) // 2
-        z0 = z + jnp.where(i % 2 == 1, -half, half)
-        return z0, jnp.logical_and(z0 >= 0, z0 < nz)
-
-    def along_z(w, i, sending):
-        z0, valid = layer(i)
-        away = z0 != z
-
-        @pl.when(valid)
-        def _():
-            mine = z0 * nx + x
-
-            def both(k, block):
-                go(w, k, block, UP, z0 <= z, sending)
-                go(w, k, block, DOWN, z0 >= z, sending)
-
-            if sending:
-                @pl.when(away)
-                def _():
-                    arrive(w, 0, mine)
-            both(0, mine)
-            go(w, 0, mine, RIGHT, yes, sending)
-            go(w, 0, mine, LEFT, yes, sending)
-            level = jnp.logical_not(away)
-
-            @pl.loop(0, nx)
-            def _(j):
-                x0 = (x + j) % nx
+        beside = z + jnp.where(i % 2 == 1, -((i + 1) // 2), i // 2)
+        beyond = jnp.where(z < nz // 2, z + i - near, z - i + near)
+        return jnp.where(i <= 2 * near, beside, beyond)
+
+    def order(q):
+        return ((y + 1) * (nz // ny) + q) % nz
+
+    def spread_z(w, k, block, z0, sending):
+        go(w, k, block, UP, z0 <= z, sending)
+        go(w, k, block, DOWN, z0 >= z, sending)
+
+    def along_z(w, k, i, sending):
+        z0 = layer(i)
+
+        @pl.when(i > 0)
+        def _():
+            def relay(block):
                 if sending:
-                    @pl.when(jnp.logical_or(away, x != x0))
-                    def _():
-                        arrive(w, 1, z0 * nx + x0)
-                go(w, 1, z0 * nx + x0, RIGHT, jnp.logical_and(level, x0 <= x), sending)
-                go(w, 1, z0 * nx + x0, LEFT, jnp.logical_and(level, x0 >= x), sending)
-                both(1, z0 * nx + x0)
+                    arrive(w, k, block)
+                spread_z(w, k, block, z0, sending)
+            if k == 0:
+                relay(z0 * nx + x)
+                go(w, 0, z0 * nx + x, RIGHT, yes, sending)
+                go(w, 0, z0 * nx + x, LEFT, yes, sending)
+            else:
+                @pl.loop(0, nx)
+                def _(j):
+                    relay(z0 * nx + (x + j) % nx)
 
     def sides(body):
         for dist in range(1, nx):
@@ -212,31 +206,37 @@
                 def _(sign=sign, x0=x0):
                     body(x0, RIGHT if sign < 0 else LEFT)
 
-    def along_x(w, i, sending):
-        z0, valid = layer(i)
-
-        @pl.when(valid)
-        def _():
-            def body(x0, way):
-                if sending:
-                    arrive(w, 0, z0 * nx + x0)
-                go(w, 0, z0 * nx + x0, way, yes, sending)
-            sides(body)
+    def along_x(w, z0, sending):
+        def body(x0, way):
+            if sending:
+                arrive(w, 0, z0 * nx + x0)
+            go(w, 0, z0 * nx + x0, way, yes, sending)
+        sides(body)
 
     def step(w, i):
-        @pl.when(i == 1)
+        @pl.when(i == 0)
         def _():
             row(w)
 
-        @pl.when(i < steps)
-        def _():
-            along_z(w, i, True)
-        along_x(w, i - 1, True)
-
-    def pump(w, lo=1, hi=steps + 1):
+        @pl.when(jnp.logical_and(i > 0, i < steps))
+        def _():
+            along_z(w, 0, i, True)
+
+        @pl.when(i >= steps)
+        def _():
+            along_z(w, 1, i - steps + 1, True)
+
+    total_steps = 2 * steps - 1
+
+    def pump(w, lo=0, hi=total_steps):
         @pl.loop(lo, hi)
         def _(i):
             step(w, i)
+
+    def across(w):
+        @pl.loop(0, steps)
+        def _(i):
+            along_x(w, layer(i), True)
 
     def spaced(move, lo, hi):
         def hook(j, total):
@@ -250,18 +250,21 @@
     def during(w, lo, hi):
         return spaced(lambda i: step(w, i), lo, hi)
 
-    def begin(w):
-        loads[w].wait()
+    def begin(w, sending=True):
+        if sending:
+            loads[w].wait()
         for k in (1, 0):
-            for way in (RIGHT, LEFT, UP, DOWN):
-                go(w, k, fs, way, yes, True)
-
-    def row(w):
+            go(w, k, fs, RIGHT, yes, sending)
+            go(w, k, fs, LEFT, yes, sending)
+            spread_z(w, k, fs, z, sending)
+
+    def row(w, sending=True):
         def body(x0, way):
             block = z * nx + x0
-            arrive(w, 1, block)
-            for to in (way, UP, DOWN):
-                go(w, 1, block, to, yes, True)
+            if sending:
+                arrive(w, 1, block)
+            go(w, 1, block, way, yes, sending)
+            spread_z(w, 1, block, z, sending)
         sides(body)
 
     def fcopy(w, p, block, src, target, sem):
@@ -285,55 +288,59 @@
             for way in (RIGHT, LEFT):
                 fgo(w, p, fs, source(w, p), way, cond, sending)
 
-    def begin_fz(w, sending=True):
+    def begin_fb(w, sending=True):
         fgo(w, 1, fs, source(w, 1), UP, up_in, sending)
         fgo(w, 1, fs, source(w, 1), DOWN, down_in, sending)
+
+    def begin_fa(w, lo, hi, sending=True):
         for e, end in enumerate((0, nz - 1)):
-            run(z != end, fcopy(w, 0, fs, source(w, 0), end * nx + x, ffar.at[w, e]), sending)
-
-    def frelay(w, i, sending=True):
-        z0, valid = layer(i)
+            apart = abs(z - end)
+            run(
+                jnp.logical_and(apart >= lo, apart <= hi),
+                fcopy(w, 0, fs, source(w, 0), end * nx + x, ffar.at[w, e]), sending,
+            )
+
+    def frelay(w, i, p):
+        @pl.when(inside if p else outside)
+        def _():
+            frelay_part(w, layer(i), p)
+
+    def frelay_part(w, z0, p, sending=True):
         block = z0 * nx + x
-
-        @pl.when(jnp.logical_and(valid, z0 != z))
-        def _():
-            def body(p):
-                ref = held(w, p, block)
+        ref = held(w, p, block)
+
+        @pl.when(z0 != z)
+        def _():
+            if sending:
+                farrive(w, p, block)
+            if p:
+                fgo(w, p, block, ref, UP, jnp.logical_and(z0 < z, up_in), sending)
+                fgo(w, p, block, ref, DOWN, jnp.logical_and(z0 > z, down_in), sending)
+            fgo(w, p, block, ref, RIGHT, yes, sending)
+            fgo(w, p, block, ref, LEFT, yes, sending)
+
+    def fside(w, z0, sending=True):
+        def part(p):
+            def body(x0, way):
+                block = z0 * nx + x0
                 if sending:
                     farrive(w, p, block)
-                if p:
-                    fgo(w, p, block, ref, UP, jnp.logical_and(z0 < z, up_in), sending)
-                    fgo(w, p, block, ref, DOWN, jnp.logical_and(z0 > z, down_in), sending)
-                fgo(w, p, block, ref, RIGHT, yes, sending)
-                fgo(w, p, block, ref, LEFT, yes, sending)
-            each_part(body)
-
-    def fside(w, i, sending=True):
-        z0, valid = layer(i)
-
-        @pl.when(valid)
-        def _():
-            def part(p):
-                def body(x0, way):
-                    block = z0 * nx + x0
-                    if sending:
-                        farrive(w, p, block)
-                    fgo(w, p, block, held(w, p, block), way, yes, sending)
-                sides(body)
-            each_part(part)
-
-    def frelays(w, lo, hi):
-        @pl.loop(lo, hi)
-        def _(i):
-            frelay(w, i)
-
-    def fduring(w, lo, hi):
-        return spaced(lambda i: frelay(w, i), lo, hi)
+                fgo(w, p, block, held(w, p, block), way, yes, sending)
+            sides(body)
+        each_part(part)
+
+    def fdo(*list_):
+        def hook(j, total):
+            for n, (w, i, p) in enumerate(list_):
+                @pl.when(j == n * total // len(list_))
+                def _(w=w, i=i, p=p):
+                    frelay(w, i, p)
+        return hook
 
     def fsides(w):
         @pl.loop(0, steps)
         def _(i):
-            fside(w, i)
+            fside(w, layer(i))
 
     def send(ref, send, recv, to):
         return pltpu.make_async_remote_copy(
@@ -392,7 +399,7 @@
                 normed[s, at, cols] = (v * scale * gain[:, cols]).astype(BF16)
             hook(m, rows // high)
 
-    mt = 256 if rows % 256 == 0 else rows
+    mt = rows
 
     def none(j, total):
         pass
@@ -417,90 +424,110 @@
         t = block // per
         return t // 2, t % 2, block % per
 
-    def out_block(weights, act, seqs, part, sib, ssend, srecv, block):
-        for s in range(seqs):
-            @pl.loop(0, rows // mt)
-            def _(m):
-                at = pl.ds(pl.multiple_of(m * mt, mt), mt)
-                part[block, s, at, :] = jnp.dot(
-                    act[s, at, :], weights[block], preferred_element_type=F32
-                ).astype(BF16)
+    def out_block(weights, act, part, sib, ssend, srecv, s, block):
+        @pl.loop(0, rows // mt)
+        def _(m):
+            at = pl.ds(pl.multiple_of(m * mt, mt), mt)
+            part[block, s, at, :] = jnp.dot(
+                act[s, at, :], weights[block], preferred_element_type=F32
+            ).astype(BF16)
         yo, co, k = owner(block)
-        run(co != core, mate_copy(part, sib, ssend, srecv, block), True)
-
-    def mate_copy(part, sib, ssend, srecv, block):
+        run(co != core, mate_copy(part, sib, ssend, srecv, s, block), True)
+
+    def mate_copy(part, sib, ssend, srecv, s, block):
         yo, co, k = owner(block)
         slot = yo * per + k
-        return send((part.at[block], sib.at[slot]), ssend.at[slot], srecv.at[slot], {"tp": mate})
-
-    def home_copy(part, s, rs, psend, precv, block, rel):
+        return send((part.at[block, s], sib.at[slot, s]), ssend.at[slot, s], srecv.at[slot, s], {"tp": mate})
+
+    def home_copy(part, rs, psend, precv, s, block):
         yo, co, k = owner(block)
-        to = {"tp": yo * 2 + core} if rel == 0 else {"fs": pair, "tp": yo * 2 + core}
-        return send((part.at[block, s], rs.at[rel, y, k]), psend.at[rel, yo, k], precv.at[rel, y, k], to)
-
-    def combine(seqs, part, sib, rs, srecv, psend, precv, block):
+        return send(
+            (part.at[block, s], rs.at[y, k, s]), psend.at[yo, k, s], precv.at[y, k, s], {"tp": yo * 2 + core}
+        )
+
+    high = 128
+
+    def row_tiles(body):
+        @pl.loop(0, rows // high)
+        def _(m):
+            body(pl.ds(pl.multiple_of(m * high, high), high))
+
+    def combine(part, sib, rs, srecv, psend, precv, s, block):
         yo, co, k = owner(block)
         slot = yo * per + k
 
         @pl.when(co == core)
         def _():
-            got(sib.at[slot], srecv.at[slot])
-            high = 128
-            for s in reversed(range(seqs)):
-                @pl.loop(0, rows // high)
-                def _(m):
-                    at = pl.ds(pl.multiple_of(m * high, high), high)
-                    part[block, s, at, :] = (
-                        part[block, s, at, :].astype(F32) + sib[slot, s, at, :].astype(F32)
-                    ).astype(BF16)
-                run(yes if s else yo != y, home_copy(part, s, rs, psend, precv, block, s), True)
+            got(sib.at[slot, s], srecv.at[slot, s])
+
+            def add(at):
+                part[block, s, at, :] = (
+                    part[block, s, at, :].astype(F32) + sib[slot, s, at, :].astype(F32)
+                ).astype(BF16)
+            row_tiles(add)
+            run(yo != y, home_copy(part, rs, psend, precv, s, block), True)
 
     def sent_home(seqs, part, sib, rs, ssend, srecv, psend, precv):
         @pl.loop(0, n_fs)
         def _(block):
             yo, co, k = owner(block)
-            run(co != core, mate_copy(part, sib, ssend, srecv, block), False)
             for s in range(seqs):
-                run(
-                    co == core if s else jnp.logical_and(co == core, yo != y),
-                    home_copy(part, s, rs, psend, precv, block, s), False,
-                )
-
-    def add_up(base, seqs, part, rs, precv, dst):
-        for rel in range(seqs):
-            for yy in (ypeers if rel == 0 else ypeers + [y]):
-                for k in range(per):
-                    got(rs.at[rel, yy, k], precv.at[rel, yy, k])
-        high = 128
-
-        @pl.loop(0, rows // high)
-        def _(m):
-            at = pl.ds(pl.multiple_of(m * high, high), high)
+                run(co != core, mate_copy(part, sib, ssend, srecv, s, block), False)
+                run(jnp.logical_and(co == core, yo != y), home_copy(part, rs, psend, precv, s, block), False)
+
+    def collected(rs, precv):
+        for k in range(per):
+            for yy in ypeers:
+                got(rs.at[yy, k, 0], precv.at[yy, k, 0])
+
+    def share(part, rs, k, s, at):
+        total = part[tp * per + k, s, at, :].astype(F32)
+        for yy in ypeers:
+            total = total + rs[yy, k, s, at, :].astype(F32)
+        return total
+
+    def add_up(base, part, rs, dst, far):
+        def add(at):
             for k in range(per):
                 cols = slice(k * wide, (k + 1) * wide)
-                total = part[tp * per + k, 0, at, :].astype(F32)
-                for rel in range(seqs):
-                    for yy in (ypeers if rel == 0 else ypeers + [y]):
-                        total = total + rs[rel, yy, k, at, :].astype(F32)
+                total = share(part, rs, k, 0, at)
+                if far is not None:
+                    total = total + far[k, at, :].astype(F32)
                 dst[at, cols] = (base[at, cols].astype(F32) + total).astype(BF16)
+        row_tiles(add)
+
+    def cross_copy(k):
+        return send((part2.at[tp * per + k, 1], far2.at[k]), far_send.at[k], far_recv.at[k], {"fs": pair})
+
+    def cross():
+        for k in range(per):
+            for yy in ypeers:
+                got(rs2.at[yy, k, 1], p2_recv.at[yy, k, 1])
+
+            def add(at):
+                part2[tp * per + k, 1, at, :] = share(part2, rs2, k, 1, at).astype(BF16)
+            row_tiles(add)
+            cross_copy(k).start()
+
+    def crossed():
+        for k in range(per):
+            got(far2.at[k], far_recv.at[k])
 
     def sweep(move, form, merge):
-        @pl.loop(0, steps + 2)
-        def _(i):
-            move(i)
-
-            def blocks(i, body):
+        @pl.loop(0, nz + 2)
+        def _(q):
+            move(q)
+
+            def blocks(q, body):
                 @pl.loop(0, nx)
                 def _(j):
-                    i0 = jnp.where(j == 0, i, i - 1)
-                    z0, good = layer(i0)
-                    good = jnp.logical_and(good, jnp.logical_and(i0 >= 0, i0 < steps))
-
-                    @pl.when(good)
+                    at = jnp.where(j == 0, q, q - 1)
+
+                    @pl.when(jnp.logical_and(at >= 0, at < nz))
                     def _():
-                        body(z0 * nx + (x + j) % nx)
-            blocks(i, form)
-            blocks(i - 1, merge)
+                        body(order(at) * nx + (x + j) % nx)
+            blocks(q, form)
+            blocks(q - 1, merge)
 
     tok_sems = (tok_sib, tok_y, tok_recv)
     st_sems = (st_sib, st_y, st_recv)
@@ -512,16 +539,21 @@
     pump(0)
     begin(2)
     ag_relay(tok, 0, tok_sib, tok_recv)
-    pump(1, 1, 3)
+    pump(1)
+    begin(3)
+    begin_fb(0)
     ag_done(tok, 0, tok_recv)
-    norm(tok, 0, mix_gain, during(1, 3, 6))
-    project(w0, 0, outer, during(1, 6, steps + 1))
-    begin(3)
-    project(w1, 0, inner, during(2, 1, 4))
-    pump(2, 4)
+    norm(tok, 0, mix_gain, during(2, 0, 2))
+    across(0)
+    project(w0, 0, outer, during(2, 2, total_steps))
+    across(1)
+    project(w1, 0, inner, during(3, 0, steps))
     begin_fx(0)
-    begin_fz(0)
-    project(w2, 0, signal, during(3, 1, 3))
+    across(2)
+    project(w2, 0, signal, during(3, steps, total_steps))
+    begin_fa(0, 1, 1)
+    frelay(0, 1, 1)
+    frelay(0, 2, 1)
 
     def mixer(index, start, size):
         cols = pl.ds(start, size)
@@ -530,42 +562,62 @@
         outer[0, :, cols] = (outer[0, :, cols].astype(F32) * causal(v, taps, mix_bias[:, cols])).astype(BF16)
     tiles(outer.shape[2], 128, mixer)
 
-    def move1(i):
-        @pl.when(jnp.logical_and(i >= 3, i <= steps))
-        def _():
-            step(3, i)
+    def move1(q):
+        @pl.when(jnp.logical_and(q >= 1, q <= nz))
+        def _():
+            along_x(3, order(q - 1), True)
     sweep(
         move1,
-        lambda b: out_block(w3, outer, 1, part1, sib1, s1_send, s1_recv, b),
-        lambda b: combine(1, part1, sib1, rs1, s1_recv, p1_send, p1_recv, b),
+        lambda b: out_block(w3, outer, part1, sib1, s1_send, s1_recv, 0, b),
+        lambda b: combine(part1, sib1, rs1, s1_recv, p1_send, p1_recv, 0, b),
     )
+    begin_fb(1)
+    begin_fa(0, 2, nz)
     begin_fx(1)
-    frelays(0, 1, 3)
-    add_up(tok.at[0, tp], 1, part1, rs1, p1_recv, state.at[0, tp])
+    frelay(0, 3, 1)
+    collected(rs1, p1_recv)
+    add_up(tok.at[0, tp], part1, rs1, state.at[0, tp], None)
     to_pair = send((state.at[0, tp], state.at[1, tp]), st_z.at[0], st_recv.at[1, tp], {"fs": pair})
     to_pair.start()
     ag_out(state, 0, *st_sems)
-    begin_fz(1)
-    frelays(0, 3, steps)
+    begin_fb(2)
+    frelay(1, 1, 1)
+    frelay(1, 2, 1)
+    frelay(0, 1, 0)
+    frelay(0, 2, 0)
+    frelay(0, 3, 0)
     ag_relay(state, 0, st_sib, st_recv)
-    frelays(1, 1, 3)
+    begin_fa(1, 1, 1)
+    frelay(1, 3, 1)
     got(state.at[1, tp], st_recv.at[1, tp])
     ag_out(state, 1, *st_sems)
-    begin_fx(2)
-    begin_fz(2)
     ag_done(state, 0, st_recv)
     norm(state, 0, ffn_gain, none)
     for w in range(3):
         own_f(w, False)
     fsides(0)
-    project(f0, 0, gate, fduring(1, 3, 5))
+    project(f0, 0, gate, none)
+    begin_fa(1, 2, 2)
+    frelay(1, 1, 0)
+    begin_fa(1, 3, nz)
+    frelay(1, 2, 0)
     ag_relay(state, 1, st_sib, st_recv)
     ag_done(state, 1, st_recv)
-    norm(state, 1, ffn_gain, fduring(1, 5, steps))
-    project(f0, 1, gate, fduring(2, 1, 3))
+    frelay(1, 3, 0)
+    begin_fx(2)
+    begin_fa(2, 1, 1)
+    norm(state, 1, ffn_gain, none)
+    frelay(2, 1, 1)
+    frelay(2, 2, 1)
+    project(f0, 1, gate, none)
+    begin_fa(2, 2, 2)
+    frelay(2, 3, 1)
     fsides(1)
+    begin_fa(2, 3, nz)
     project(f1, 0, value, none)
+    frelay(2, 1, 0)
     project(f1, 1, value, none)
+    frelay(2, 2, 0)
     shift = jnp.where(outside, big, 0)
 
     @pl.loop(0, jnp.where(outside, small, big) // 128)
@@ -577,39 +629,51 @@
             v = causal(value[s, :, cols].astype(F32), [ffn_taps[j:j + 1, at] for j in range(3, 6)], ffn_bias[1:2, at])
             gate[s, :, cols] = (g / (1.0 + jnp.exp(-g)) * v).astype(BF16)
 
-    def move2(i):
-        @pl.when(jnp.logical_and(i >= 3, i < steps))
-        def _():
-            frelay(2, i)
-
-        @pl.when(jnp.logical_and(i >= 1, i <= steps))
-        def _():
-            fside(2, i - 1)
-    sweep(
-        move2,
-        lambda b: out_block(f2, gate, 2, part2, sib2, s2_send, s2_recv, b),
-        lambda b: combine(2, part2, sib2, rs2, s2_recv, p2_send, p2_recv, b),
-    )
-    add_up(state.at[0, tp], 2, part2, rs2, p2_recv, out)
+    frelay(2, 3, 0)
+
+    def move2(q):
+        @pl.when(jnp.logical_and(q >= 1, q <= nz))
+        def _():
+            fside(2, order(q - 1))
+
+    def sweep2(s):
+        sweep(
+            move2 if s else (lambda q: None),
+            lambda b: out_block(f2, gate, part2, sib2, s2_send, s2_recv, s, b),
+            lambda b: combine(part2, sib2, rs2, s2_recv, p2_send, p2_recv, s, b),
+        )
+    sweep2(1)
+    sweep2(0)
+    cross()
+    crossed()
+    collected(rs2, p2_recv)
+    add_up(state.at[0, tp], part2, rs2, out, far2)
 
     to_pair.wait_send()
     ag_sent(tok, 0, *tok_sems)
     ag_sent(state, 0, *st_sems)
     ag_sent(state, 1, *st_sems)
+    for k in range(per):
+        cross_copy(k).wait_send()
     sent_home(1, part1, sib1, rs1, s1_send, s1_recv, p1_send, p1_recv)
     sent_home(2, part2, sib2, rs2, s2_send, s2_recv, p2_send, p2_recv)
     for w in range(4):
+        begin(w, False)
+        row(w, False)
+
         @pl.loop(0, steps)
         def _(i):
-            along_z(w, i, False)
+            along_z(w, 0, i, False)
+            along_z(w, 1, i, False)
             along_x(w, i, False)
     for w in range(3):
         begin_fx(w, False)
-        begin_fz(w, False)
+        begin_fb(w, False)
+        begin_fa(w, 1, nz, False)
 
         @pl.loop(0, steps)
         def _(i):
-            frelay(w, i, False)
+            each_part(lambda p: frelay_part(w, i, p, False))
             fside(w, i, False)
 
 
@@ -657,10 +721,11 @@
                 pltpu.VMEM((2, rows, big), BF16),
                 pltpu.VMEM((n_fs, 1, rows, wide), BF16),
                 pltpu.VMEM((ny * per, 1, rows, wide), BF16),
-                pltpu.VMEM((1, ny, per, rows, wide), BF16),
+                pltpu.VMEM((ny, per, 1, rows, wide), BF16),
                 pltpu.VMEM((n_fs, 2, rows, wide), BF16),
                 pltpu.VMEM((ny * per, 2, rows, wide), BF16),
-                pltpu.VMEM((2, ny, per, rows, wide), BF16),
+                pltpu.VMEM((ny, per, 2, rows, wide), BF16),
+                pltpu.VMEM((per, rows, wide), BF16),
                 dma((8,)),
                 dma((4, 2, n_fs, 4)),
                 dma((4, 2, n_fs)),
@@ -669,8 +734,9 @@
                 dma((3, n_fs)),
                 dma((1, n_tp)), dma((1, ny)), dma((1, n_tp)),
                 dma((2, n_tp)), dma((2, ny)), dma((1,)), dma((2, n_tp)),
-                dma((ny * per,)), dma((ny * per,)), dma((1, ny, per)), dma((1, ny, per)),
-                dma((ny * per,)), dma((ny * per,)), dma((2, ny, per)), dma((2, ny, per)),
+                dma((ny * per, 1)), dma((ny * per, 1)), dma((ny, per, 1)), dma((ny, per, 1)),
+                dma((ny * per, 2)), dma((ny * per, 2)), dma((ny, per, 2)), dma((ny, per, 2)),
+                dma((per,)), dma((per,)),
             ],
             compiler_params=pltpu.CompilerParams(
                 collective_id=0, has_side_effects=True, vmem_limit_bytes=67043328

time: 289 us -> 254 us (0.88)
  the two profiles are of different devices: /device:TPU:3 before, /device:TPU:19 now
where the time goes in v2:
time: 254 us; the launch traced here: 253 us
  Pallas kernels  250 us (98%)
  local copies, waits for them, and re-layouts  3.47 us (1%)
    pallas_call x1, Pallas kernels, on_device(): pl.pallas_call(functools.partial(kernel, n_fs, n_tp), out_shape=jax.Shape...  250 us

profile of v2, /device:TPU:19, one launch (start us, length us, event | category | flops | bytes accessed | tf_op | source)
XLA Modules:
  0.0 253.3 jit_solution(2943040670915488979)
XLA Ops:
  0.0 0.8 copy.16
  0.8 0.6 reshape.3.ffn_taps
  1.4 249.8 %shard_map.136 = bf16[768,512]{1,0:T(8,128)(2,1)} custom-call(bf16[768,512]{1,0:T(8,128)(2,1)} %tok_in.1, bf16[256,512]{1,0:T(8,128)(2,1)} %og.1, bf16[256,512]{1,0:T(8,128)(2,1)} %ig.1, bf16[256,512]{1,0:T(8,128)(2,1)} %si.1, bf16[512,256]{1,0:T(8,128)(2,1)} %mo.1, bf16[256,1408]{1,0:T(8,128)(2,1)} %ug.1, bf16[256,1408]{1,0:T(8,128)(2,1)} %uv.1, ...), custom_call_target="tpu_custom_call" | custom-call | tf_op jit(solution)/shard_map/pallas_call | solution.py:704
  251.3 2.1 copy.18

commit v3 on v2

--- a/solution.py
+++ b/solution.py
@@ -179,10 +179,9 @@
         go(w, k, block, UP, z0 <= z, sending)
         go(w, k, block, DOWN, z0 >= z, sending)
 
-    def along_z(w, k, i, sending):
-        z0 = layer(i)
-
-        @pl.when(i > 0)
+    def along_z(w, k, z0, sending):
+
+        @pl.when(z0 != z)
         def _():
             def relay(block):
                 if sending:
@@ -220,11 +219,11 @@
 
         @pl.when(jnp.logical_and(i > 0, i < steps))
         def _():
-            along_z(w, 0, i, True)
+            along_z(w, 0, layer(i), True)
 
         @pl.when(i >= steps)
         def _():
-            along_z(w, 1, i - steps + 1, True)
+            along_z(w, 1, layer(i - steps + 1), True)
 
     total_steps = 2 * steps - 1
 
@@ -293,12 +292,45 @@
         fgo(w, 1, fs, source(w, 1), DOWN, down_in, sending)
 
     def begin_fa(w, lo, hi, sending=True):
+        stage = (z - (y + 1) * (nz // ny)) % nz + 1
         for e, end in enumerate((0, nz - 1)):
-            apart = abs(z - end)
+            turn = stage if w == 2 else abs(z - end)
             run(
-                jnp.logical_and(apart >= lo, apart <= hi),
+                jnp.logical_and(z != end, jnp.logical_and(turn >= lo, turn <= hi)),
                 fcopy(w, 0, fs, source(w, 0), end * nx + x, ffar.at[w, e]), sending,
             )
+
+    outer_side = jnp.where(z < nz // 2, 0, nz - 1)
+
+    def fz():
+        @pl.when(inside)
+        def _():
+            block = outer_side * nx + x
+            ref = held(2, 1, block)
+            farrive(2, 1, block)
+            fgo(2, 1, block, ref, UP, outer_side == 0, True)
+            fgo(2, 1, block, ref, DOWN, outer_side != 0, True)
+
+    def fnext(q, p):
+        z0 = order(q)
+        block = z0 * nx + x
+        mine = z0 == z
+
+        def both(src, cond):
+            for way in (RIGHT, LEFT):
+                fgo(2, p, block, src, way, cond, True)
+
+        @pl.when(inside if p else outside)
+        def _():
+            both(source(2, p), mine)
+            waits = jnp.logical_not(mine)
+            if p:
+                waits = jnp.logical_and(waits, z0 != outer_side)
+
+            @pl.when(waits)
+            def _():
+                farrive(2, p, block)
+            both(held(2, p, block), jnp.logical_not(mine))
 
     def frelay(w, i, p):
         @pl.when(inside if p else outside)
@@ -528,6 +560,33 @@
                         body(order(at) * nx + (x + j) % nx)
             blocks(q, form)
             blocks(q - 1, merge)
+
+    def mixer_sent():
+        ag_sent(tok, 0, *tok_sems)
+        sent_home(1, part1, sib1, rs1, s1_send, s1_recv, p1_send, p1_recv)
+        for w in range(4):
+            begin(w, False)
+            row(w, False)
+
+            @pl.loop(0, nz)
+            def _(i):
+                along_z(w, 0, i, False)
+                along_z(w, 1, i, False)
+                along_x(w, i, False)
+
+    def ffn_sent():
+        to_pair.wait_send()
+        ag_sent(state, 0, *st_sems)
+        ag_sent(state, 1, *st_sems)
+        for w in range(3):
+            begin_fx(w, False)
+            begin_fb(w, False)
+            begin_fa(w, 1, nz, False)
+
+            @pl.loop(0, nz)
+            def _(i):
+                each_part(lambda p: frelay_part(w, i, p, False))
+                fside(w, i, False)
 
     tok_sems = (tok_sib, tok_y, tok_recv)
     st_sems = (st_sib, st_y, st_recv)
@@ -586,95 +645,76 @@
     frelay(0, 1, 0)
     frelay(0, 2, 0)
     frelay(0, 3, 0)
+    mixer_sent()
     ag_relay(state, 0, st_sib, st_recv)
     begin_fa(1, 1, 1)
     frelay(1, 3, 1)
     got(state.at[1, tp], st_recv.at[1, tp])
     ag_out(state, 1, *st_sems)
+    begin_fa(1, 2, 2)
     ag_done(state, 0, st_recv)
     norm(state, 0, ffn_gain, none)
     for w in range(3):
         own_f(w, False)
     fsides(0)
     project(f0, 0, gate, none)
-    begin_fa(1, 2, 2)
+    fz()
     frelay(1, 1, 0)
     begin_fa(1, 3, nz)
     frelay(1, 2, 0)
     ag_relay(state, 1, st_sib, st_recv)
     ag_done(state, 1, st_recv)
     frelay(1, 3, 0)
-    begin_fx(2)
-    begin_fa(2, 1, 1)
+    begin_fa(2, 1, 2)
+    for q in range(nz):
+        fnext(q, 1)
     norm(state, 1, ffn_gain, none)
-    frelay(2, 1, 1)
-    frelay(2, 2, 1)
     project(f0, 1, gate, none)
-    begin_fa(2, 2, 2)
-    frelay(2, 3, 1)
+    begin_fa(2, 3, nz)
     fsides(1)
-    begin_fa(2, 3, nz)
+    fnext(0, 0)
     project(f1, 0, value, none)
-    frelay(2, 1, 0)
+    fnext(1, 0)
     project(f1, 1, value, none)
-    frelay(2, 2, 0)
+    fnext(2, 0)
     shift = jnp.where(outside, big, 0)
 
     @pl.loop(0, jnp.where(outside, small, big) // 128)
     def _(i):
+        @pl.when(i == 1)
+        def _():
+            fnext(3, 0)
         cols = pl.ds(pl.multiple_of(i * 128, 128), 128)
         at = pl.ds(pl.multiple_of(shift + i * 128, 128), 128)
         for s in range(2):
-            g = causal(gate[s, :, cols].astype(F32), [ffn_taps[j:j + 1, at] for j in range(3)], ffn_bias[0:1, at])
-            v = causal(value[s, :, cols].astype(F32), [ffn_taps[j:j + 1, at] for j in range(3, 6)], ffn_bias[1:2, at])
+            g = causal(gate[s, :, cols].astype(F32), [ffn_taps[j, 0:1, at] for j in range(3)], ffn_bias[0:1, at])
+            v = causal(value[s, :, cols].astype(F32), [ffn_taps[j, 1:2, at] for j in range(3)], ffn_bias[1:2, at])
             gate[s, :, cols] = (g / (1.0 + jnp.exp(-g)) * v).astype(BF16)
 
-    frelay(2, 3, 0)
-
-    def move2(q):
-        @pl.when(jnp.logical_and(q >= 1, q <= nz))
-        def _():
-            fside(2, order(q - 1))
-
-    def sweep2(s):
-        sweep(
-            move2 if s else (lambda q: None),
-            lambda b: out_block(f2, gate, part2, sib2, s2_send, s2_recv, s, b),
-            lambda b: combine(part2, sib2, rs2, s2_recv, p2_send, p2_recv, s, b),
-        )
-    sweep2(1)
-    sweep2(0)
+    def form2(s, b):
+        out_block(f2, gate, part2, sib2, s2_send, s2_recv, s, b)
+
+    def merge2(s, b):
+        combine(part2, sib2, rs2, s2_recv, p2_send, p2_recv, s, b)
+
+    @pl.loop(0, nz)
+    def _(q):
+        z0 = order(q)
+        fside(2, z0)
+        for act in (form2, merge2):
+            for s in (1, 0):
+                @pl.loop(0, nx)
+                def _(j):
+                    act(s, z0 * nx + (x + j) % nx)
     cross()
+    ffn_sent()
     crossed()
     collected(rs2, p2_recv)
     add_up(state.at[0, tp], part2, rs2, out, far2)
 
-    to_pair.wait_send()
-    ag_sent(tok, 0, *tok_sems)
-    ag_sent(state, 0, *st_sems)
-    ag_sent(state, 1, *st_sems)
+    sent_home(2, part2, sib2, rs2, s2_send, s2_recv, p2_send, p2_recv)
     for k in range(per):
         cross_copy(k).wait_send()
-    sent_home(1, part1, sib1, rs1, s1_send, s1_recv, p1_send, p1_recv)
-    sent_home(2, part2, sib2, rs2, s2_send, s2_recv, p2_send, p2_recv)
-    for w in range(4):
-        begin(w, False)
-        row(w, False)
-
-        @pl.loop(0, steps)
-        def _(i):
-            along_z(w, 0, i, False)
-            along_z(w, 1, i, False)
-            along_x(w, i, False)
-    for w in range(3):
-        begin_fx(w, False)
-        begin_fb(w, False)
-        begin_fa(w, 1, nz, False)
-
-        @pl.loop(0, steps)
-        def _(i):
-            each_part(lambda p: frelay_part(w, i, p, False))
-            fside(w, i, False)
 
 
 def solution(mesh):
@@ -685,12 +725,12 @@
         ffn_gain, up_gate, up_value, ffn_taps, ffn_bias, down_proj,
     ):
         rows, own = tokens.shape
-        ffn_taps = ffn_taps.reshape(6, -1)
         spare = -up_gate.shape[1] % 128
         if spare:
-            up_gate, up_value, ffn_taps, ffn_bias = (
-                jnp.pad(a, ((0, 0), (0, spare))) for a in (up_gate, up_value, ffn_taps, ffn_bias)
+            up_gate, up_value, ffn_bias = (
+                jnp.pad(a, ((0, 0), (0, spare))) for a in (up_gate, up_value, ffn_bias)
             )
+            ffn_taps = jnp.pad(ffn_taps, ((0, 0), (0, 0), (0, spare)))
             down_proj = jnp.pad(down_proj, ((0, spare), (0, 0)))
         weights = (outer_gate, inner_gate, signal_in, mix_out)
         chan, hidden = outer_gate.shape[1], up_gate.shape[1]
@@ -743,7 +783,7 @@
             ),
         )(
             tokens, *weights, up_gate, up_value, down_proj, mix_gain[None], ffn_gain[None], mix_taps, mix_bias[None],
-            ffn_taps, ffn_bias,
+            jnp.transpose(ffn_taps, (1, 0, 2)), ffn_bias,
         )
 
     return jax.shard_map(

time: 254 us -> 233 us (0.917)
  the two profiles are of different devices: /device:TPU:19 before, /device:TPU:3 now
where the time goes in v3:
time: 233 us
  Pallas kernels  231 us (99%)
    pallas_call x1, Pallas kernels, on_device(): pl.pallas_call(functools.partial(kernel, n_fs, n_tp), out_shape=jax.Shape...  231 us

profile of v3, /device:TPU:3, one launch (start us, length us, event | category | flops | bytes accessed | tf_op | source)
XLA Modules:
  0.0 232.7 jit_solution(1044648675588191348)
XLA Ops:
  0.0 230.6 %shard_map.136 = bf16[768,512]{1,0:T(8,128)(2,1)} custom-call(bf16[768,512]{1,0:T(8,128)(2,1)} %tok_in.1, bf16[256,512]{1,0:T(8,128)(2,1)} %og.1, bf16[256,512]{1,0:T(8,128)(2,1)} %ig.1, bf16[256,512]{1,0:T(8,128)(2,1)} %si.1, bf16[512,256]{1,0:T(8,128)(2,1)} %mo.1, bf16[256,1408]{1,0:T(8,128)(2,1)} %ug.1, bf16[256,1408]{1,0:T(8,128)(2,1)} %uv.1, ...), custom_call_target="tpu_custom_call" | custom-call | tf_op jit(solution)/shard_map/pallas_call | solution.py:744
  230.7 2.1 copy.16

commit v4 on v3

--- a/solution.py
+++ b/solution.py
@@ -44,7 +44,7 @@
     w0, w1, w2, w3, f0, f1, f2,
     tok, normed, state, outer, inner, signal, gate, value,
     part1, sib1, rs1, part2, sib2, rs2, far2,
-    load_sem, send_sem, recv_sem, fsend, ffar, frecv,
+    load_sem, send_sem, row_sem, recv_sem, fsend, ffar, frecv,
     tok_sib, tok_y, tok_recv, st_sib, st_y, st_z, st_recv,
     s1_send, s1_recv, p1_send, p1_recv, s2_send, s2_recv, p2_send, p2_recv, far_send, far_recv,
 ):
@@ -127,25 +127,25 @@
 
     for w in range(3):
         own_f(w, True)
-    if small < big:
-        @pl.when(outside)
-        def _():
-            for w in range(2):
-                fbufs[w][:, :, small:big] = jnp.zeros((n_fs, f0.shape[1], big - small), BF16)
-            f2[:, small:big, :] = jnp.zeros((n_fs, big - small, wide), BF16)
     pl.semaphore_wait(barrier, expected)
 
     def cut(w):
         r = bufs[w].shape[1]
         a = max(16, (r * 13 // 16) // 16 * 16)
         return ((0, a), (a, r - a))
+
+    def slot(block, way, wide_row):
+        z0, x0 = block // nx, block % nx
+        if wide_row:
+            return jnp.where(z0 == z, x0 * 4 + way, nx * 4 + block)
+        return jnp.where(x0 == x, z0 * 4 + way, nz * 4 + block)
 
     def piece(w, k, block, way):
         start, size = cut(w)[k]
         ref = bufs[w].at[block, pl.ds(start, size)]
         return pltpu.make_async_remote_copy(
             src_ref=ref, dst_ref=ref,
-            send_sem=send_sem.at[w, k, block, way], recv_sem=recv_sem.at[w, k, block],
+            send_sem=(row_sem if k else send_sem).at[w, slot(block, way, k)], recv_sem=recv_sem.at[w, k, block],
             device_id={"fs": ways[way][1]}, device_id_type=MESH,
         )
 
@@ -274,10 +274,10 @@
 
     def fgo(w, p, block, src, way, cond, sending):
         there, target = ways[way]
-        run(jnp.logical_and(cond, there), fcopy(w, p, block, src, target, fsend.at[w, block, way]), sending)
+        run(jnp.logical_and(cond, there), fcopy(w, p, block, src, target, fsend.at[w, slot(block, way, 0)]), sending)
 
     def farrive(w, p, block):
-        fcopy(w, p, block, held(w, p, block), fs, fsend.at[w, block, 0]).wait_recv()
+        fcopy(w, p, block, held(w, p, block), fs, fsend.at[w, 0]).wait_recv()
 
     up_in = jnp.logical_and(z + 1 >= 1, z + 1 <= nz - 2)
     down_in = jnp.logical_and(z - 1 >= 1, z - 1 <= nz - 2)
@@ -322,7 +322,8 @@
 
         @pl.when(inside if p else outside)
         def _():
-            both(source(2, p), mine)
+            if p:
+                both(source(2, p), mine)
             waits = jnp.logical_not(mine)
             if p:
                 waits = jnp.logical_and(waits, z0 != outer_side)
@@ -595,6 +596,12 @@
     begin(1)
     loads[4].wait()
     ag_out(tok, 0, *tok_sems)
+    if small < big:
+        @pl.when(outside)
+        def _():
+            for w in range(2):
+                fbufs[w][:, :, small:big] = jnp.zeros((n_fs, f0.shape[1], big - small), BF16)
+            f2[:, small:big, :] = jnp.zeros((n_fs, big - small, wide), BF16)
     pump(0)
     begin(2)
     ag_relay(tok, 0, tok_sib, tok_recv)
@@ -645,6 +652,8 @@
     frelay(0, 1, 0)
     frelay(0, 2, 0)
     frelay(0, 3, 0)
+    for way in (RIGHT, LEFT):
+        fgo(2, 0, fs, source(2, 0), way, outside, True)
     mixer_sent()
     ag_relay(state, 0, st_sib, st_recv)
     begin_fa(1, 1, 1)
@@ -741,9 +750,10 @@
         vmem = pl.BlockSpec(memory_space=pltpu.VMEM)
         dma = pltpu.SemaphoreType.DMA
         per, ny = n_fs // n_tp, n_tp // 2
+        nz, nx = grid_of(n_fs)
         return pl.pallas_call(
             functools.partial(kernel, n_fs, n_tp),
-            out_shape=jax.ShapeDtypeStruct(tokens.shape, BF16),
+            out_shape=pltpu.VMEM(tokens.shape, BF16),
             in_specs=[hbm] * 8 + [vmem] * 6,
             out_specs=vmem,
             scratch_shapes=[pltpu.VMEM((n_fs, *w.shape), BF16) for w in weights]
@@ -767,9 +777,10 @@
                 pltpu.VMEM((ny, per, 2, rows, wide), BF16),
                 pltpu.VMEM((per, rows, wide), BF16),
                 dma((8,)),
-                dma((4, 2, n_fs, 4)),
+                dma((4, 4 * nz + n_fs)),
+                dma((4, 4 * nx + n_fs)),
                 dma((4, 2, n_fs)),
-                dma((3, n_fs, 4)),
+                dma((3, 4 * nz + n_fs)),
                 dma((3, 2)),
                 dma((3, n_fs)),
                 dma((1, n_tp)), dma((1, ny)), dma((1, n_tp)),
@@ -779,7 +790,7 @@
                 dma((per,)), dma((per,)),
             ],
             compiler_params=pltpu.CompilerParams(
-                collective_id=0, has_side_effects=True, vmem_limit_bytes=67043328
+                collective_id=0, has_side_effects=True, vmem_limit_bytes=65 * 2**20 - 2**20 * 2
             ),
         )(
             tokens, *weights, up_gate, up_value, down_proj, mix_gain[None], ffn_gain[None], mix_taps, mix_bias[None],

time: 233 us -> 230 us (0.987)
  Pallas kernels: 231 us -> 228 us
where the time goes in v4:
time: 230 us; the launch traced here: 229 us
  Pallas kernels  228 us (99%)
    pallas_call x1, Pallas kernels, on_device(): pl.pallas_call(functools.partial(kernel, n_fs, n_tp), out_shape=pltpu.VME...  228 us

profile of v4, /device:TPU:3, one launch (start us, length us, event | category | flops | bytes accessed | tf_op | source)
XLA Modules:
  0.0 229.3 jit_solution(2966412650817932165)
XLA Ops:
  0.0 228.5 %shard_map.136 = bf16[768,512]{1,0:T(8,128)(2,1)S(1)} custom-call(bf16[768,512]{1,0:T(8,128)(2,1)} %tok_in.1, bf16[256,512]{1,0:T(8,128)(2,1)} %og.1, bf16[256,512]{1,0:T(8,128)(2,1)} %ig.1, bf16[256,512]{1,0:T(8,128)(2,1)} %si.1, bf16[512,256]{1,0:T(8,128)(2,1)} %mo.1, bf16[256,1408]{1,0:T(8,128)(2,1)} %ug.1, bf16[256,1408]{1,0:T(8,128)(2,1)} %uv.1, ...), custom_call_target="tpu_custom_call" | custom-call | tf_op jit(solution)/shard_map/pallas_call | solution.py:754
  228.5 0.9 copy.16
